TPU v7x, 128 devices: a whole 4x4x4 slice. The times are simulated.
128 devices in a mesh: sp: 16 (over z, x), dp: 8 (over y, core).
Axes of the slice: x: 4, y: 4, z: 4, core: 2. Of those that a mesh axis runs over, the one named last changes fastest.
Arguments:
- queries: bfloat16 [8, 2048, 2048], P('dp', 'sp'), may hold values from -9 to 9
- keys: bfloat16 [8, 2048, 512], P('dp', 'sp'), may hold values from -9 to 9
- values: bfloat16 [8, 2048, 512], P('dp', 'sp'), may hold values from -6 to 6
- out_grad: bfloat16 [8, 2048, 2048], P('dp', 'sp'), may hold values from -24 to 24
- layer_in: bfloat16 [8, 2048, 4096], P('dp', 'sp'), may hold values from -0.09375 to 0.09375
- key_weight: bfloat16 [4096, 512], P('dp'), may hold values from -0.09375 to 0.09375
- value_weight: bfloat16 [4096, 512], P('dp'), may hold values from -0.09375 to 0.09375
- query_gain: float32 [128], replicated, may hold values from 0.64 to 6.04
- key_gain: float32 [128], replicated, may hold values from 0.64 to 6.04
Outputs:
- grad_query: bfloat16 [8, 2048, 2048], P('dp', 'sp')
- grad_in: bfloat16 [8, 2048, 4096], P('dp', 'sp')
- grad_key_weight: float32 [4096, 512], P('dp')
- grad_value_weight: float32 [4096, 512], P('dp')
All inputs are finite; a program needn't handle non-finite values.
Results may differ from a plain program's by a relative error of at most 0.018.
The roundings to bfloat16 on the way count: a program that leaves them out, or rounds other values in their place, can miss the bound.
Values may be sent and summed in bfloat16 or wider, within the bound.
A program may use at most 128 MiB of HBM per device.

v0:
```python
from functools import partial
import math
import jax
import jax.numpy as jnp
from jax import lax
from jax.sharding import PartitionSpec as P

HEADS = 16
KV_HEADS = 4
HEAD_DIM = 128
GRID_W = 64
epsilon = 1e-06
rope_base = 10000.0


def sent_together(arrays, axis, dim, along):
    widths = [a.shape[along] for a in arrays]
    both = jnp.concatenate(arrays, axis=along)
    result = lax.all_gather(both, axis, axis=dim, tiled=True)
    return tuple(jnp.split(result, [sum(widths[:k]) for k in range(1, len(widths))], axis=along))


def padded_to(lines, peers):
    spare = -len(lines) % peers
    return jnp.pad(lines, [(0, spare)] + [(0, 0)] * (lines.ndim - 1))


def copy_for_each(array, axis):
    peers = lax.axis_size(axis)
    return lax.all_to_all(
        jnp.broadcast_to(array[None], (peers, *array.shape)), axis, 0, 0, tiled=True
    )


def laid_out(parts, dim):
    dims = list(parts.shape[1:])
    dims[dim] *= parts.shape[0]
    return jnp.moveaxis(parts, 0, dim).reshape(dims)


def collect(array, axis, dim):
    parts = copy_for_each(array, axis)
    return laid_out(parts, dim)


def cut_along(array, dim, peers):
    before, after = (array.shape[:dim], array.shape[dim + 1 :])
    return jnp.moveaxis(array.reshape(*before, peers, -1, *after), dim, 0)


def sum_at_owner(array, axis, dim):
    peers = lax.axis_size(axis)
    parts = lax.all_to_all(cut_along(array, dim, peers), axis, 0, 0, tiled=True)
    return jnp.sum(parts.astype(jnp.float32), axis=0)


def nested_sum(array, axes):
    lines = array.reshape(-1, array.shape[-1])
    padded = padded_to(lines, lax.axis_size(axes))
    whole = collect(sum_at_owner(padded, axes, 0).astype(jnp.bfloat16), axes, 0)
    return lax.slice_in_dim(whole, 0, len(lines)).reshape(array.shape).astype(jnp.float32)


def norm_rotate(vector, gain_vec, row_index, col_index):
    scaled = (
        vector * lax.rsqrt(jnp.mean(vector * vector, axis=-1, keepdims=True) + epsilon) * gain_vec
    )
    quarter = vector.shape[-1] // 4
    inverse = rope_base ** (-jnp.arange(quarter, dtype=jnp.float32) / quarter)
    pieces = []
    for offset, position in ((0, row_index), (2 * quarter, col_index)):
        angles = position.astype(jnp.float32)[:, None] * inverse[None, :]
        cosine = jnp.cos(angles)
        sine_part = jnp.sin(angles)
        first_half = scaled[:, offset : offset + quarter]
        second_half = scaled[:, offset + quarter : offset + 2 * quarter]
        pieces.append(first_half * cosine - second_half * sine_part)
        pieces.append(first_half * sine_part + second_half * cosine)
    return jnp.concatenate(pieces, axis=1)


def contract_cols(left_side, right_side):
    return lax.dot_general(
        left_side, right_side, (((1,), (1,)), ((), ())), preferred_element_type=jnp.float32
    )


def contract_rows(left_side, right_side):
    return lax.dot_general(
        left_side, right_side, (((0,), (0,)), ((), ())), preferred_element_type=jnp.float32
    )


def head_grads(query_rows, grad_rows, key_rows, value_rows, query_gain, key_gain):
    length = query_rows.shape[0]
    block_rows = math.gcd(length, 512)
    positions = jnp.arange(length, dtype=jnp.int32)
    row_index = positions // GRID_W
    col_index = positions % GRID_W
    q_rot, q_back = jax.vjp(
        partial(norm_rotate, gain_vec=query_gain, row_index=row_index, col_index=col_index),
        query_rows.astype(jnp.float32),
    )
    k_rot, k_back = jax.vjp(
        partial(norm_rotate, gain_vec=key_gain, row_index=row_index, col_index=col_index),
        key_rows.astype(jnp.float32),
    )
    q_bf = q_rot.astype(jnp.bfloat16)
    k_bf = k_rot.astype(jnp.bfloat16)
    score_scale = q_rot.shape[-1] ** (-0.5)

    def one_block(accums, block_index):
        k_acc, v_acc = accums
        row_start = block_index * block_rows
        q_block = lax.dynamic_slice_in_dim(q_bf, row_start, block_rows, 0)
        g_block = lax.dynamic_slice_in_dim(grad_rows, row_start, block_rows, 0)
        scores = contract_cols(q_block, k_bf) * score_scale
        shifted = jnp.exp(scores - jnp.max(scores, axis=1, keepdims=True))
        attn_probs = shifted / jnp.sum(shifted, axis=1, keepdims=True)
        probs_b = attn_probs.astype(jnp.bfloat16)
        attn_out = jnp.dot(probs_b, value_rows, preferred_element_type=jnp.float32)
        row_delta = jnp.sum(g_block.astype(jnp.float32) * attn_out, axis=1, keepdims=True)
        grad_probs = contract_cols(g_block, value_rows)
        grad_scores = (attn_probs * (grad_probs - row_delta)).astype(jnp.bfloat16)
        q_grad = jnp.dot(grad_scores, k_bf, preferred_element_type=jnp.float32) * score_scale
        k_acc = k_acc + contract_rows(grad_scores, q_block) * score_scale
        v_acc = v_acc + contract_rows(probs_b, g_block)
        return ((k_acc, v_acc), q_grad)

    zeros_init = jnp.zeros(query_rows.shape, jnp.float32)
    (k_acc, v_acc), q_grads = lax.scan(
        one_block, (zeros_init, zeros_init), jnp.arange(length // block_rows, dtype=jnp.int32)
    )
    grad_rq = q_grads.reshape(length, query_rows.shape[1])
    grad_q = q_back(grad_rq)[0].astype(jnp.bfloat16)
    grad_k = k_back(k_acc)[0].astype(jnp.bfloat16)
    return (grad_q, grad_k, v_acc.astype(jnp.bfloat16))


def on_device(
    queries, keys, values, out_grad, layer_in, key_weight, value_weight, query_gain, key_gain
):
    seq_count, tokens_here, _ = queries.shape
    model_width = layer_in.shape[2]
    group_size = HEADS // KV_HEADS
    kv_width = KV_HEADS * HEAD_DIM
    key_full, value_full = sent_together((key_weight, value_weight), "dp", 0, 1)
    query_part = queries.reshape(seq_count, tokens_here, HEADS, HEAD_DIM)
    grad_part = out_grad.reshape(seq_count, tokens_here, HEADS, HEAD_DIM)
    shape_wide = (seq_count, tokens_here, KV_HEADS, group_size, HEAD_DIM)
    key_part = jnp.broadcast_to(
        keys.reshape(seq_count, tokens_here, KV_HEADS, 1, HEAD_DIM), shape_wide
    ).reshape(seq_count, tokens_here, HEADS, HEAD_DIM)
    value_part = jnp.broadcast_to(
        values.reshape(seq_count, tokens_here, KV_HEADS, 1, HEAD_DIM), shape_wide
    ).reshape(seq_count, tokens_here, HEADS, HEAD_DIM)
    bundle = jnp.concatenate([query_part, grad_part, key_part, value_part], axis=3)
    arrived = lax.all_to_all(bundle, "sp", split_axis=2, concat_axis=1, tiled=True)
    arrived_seqs, length, head_count, _ = arrived.shape
    flat_heads = arrived.transpose(0, 2, 1, 3).reshape(
        arrived_seqs * head_count, length, 4 * HEAD_DIM
    )

    def one_item(one_head):
        grad_q, grad_k, grad_v = head_grads(
            one_head[:, :HEAD_DIM],
            one_head[:, HEAD_DIM : 2 * HEAD_DIM],
            one_head[:, 2 * HEAD_DIM : 3 * HEAD_DIM],
            one_head[:, 3 * HEAD_DIM :],
            query_gain,
            key_gain,
        )
        return jnp.concatenate([grad_q, grad_k, grad_v], axis=1)

    all_grads = lax.map(one_item, flat_heads)
    head_out = all_grads.reshape(arrived_seqs, head_count, length, 3 * HEAD_DIM).transpose(
        0, 2, 1, 3
    )
    token_grads = lax.all_to_all(head_out, "sp", split_axis=1, concat_axis=2, tiled=True)
    grad_query = token_grads[:, :, :, :HEAD_DIM].reshape(seq_count, tokens_here, HEADS * HEAD_DIM)

    def grouped(array):
        summed = jnp.sum(
            array.reshape(seq_count * tokens_here, KV_HEADS, group_size, HEAD_DIM).astype(
                jnp.float32
            ),
            axis=2,
        )
        return summed.astype(jnp.bfloat16).reshape(seq_count * tokens_here, kv_width)

    kv_grad = jnp.concatenate(
        [
            grouped(token_grads[:, :, :, HEAD_DIM : 2 * HEAD_DIM]),
            grouped(token_grads[:, :, :, 2 * HEAD_DIM :]),
        ],
        axis=1,
    )
    both_weights = jnp.concatenate([key_full, value_full], axis=1)
    grad_flat = contract_cols(kv_grad, both_weights)
    grad_in = grad_flat.astype(jnp.bfloat16).reshape(seq_count, tokens_here, model_width)
    flat_in = layer_in.reshape(seq_count * tokens_here, model_width)
    partial_sum = lax.psum_scatter(
        contract_rows(flat_in, kv_grad).astype(jnp.bfloat16), "dp", scatter_dimension=0, tiled=True
    )
    weight_grad = nested_sum(partial_sum, "sp")
    return (grad_query, grad_in, weight_grad[:, :kv_width], weight_grad[:, kv_width:])


def solution(mesh):
    in_specs = (
        P("dp", "sp", None),
        P("dp", "sp", None),
        P("dp", "sp", None),
        P("dp", "sp", None),
        P("dp", "sp", None),
        P("dp", None),
        P("dp", None),
        P(),
        P(),
    )
    out_specs = (P("dp", "sp", None), P("dp", "sp", None), P("dp", None), P("dp", None))
    return jax.shard_map(
        on_device, mesh=mesh, in_specs=in_specs, out_specs=out_specs, check_vma=False
    )
```

profile of v0, /device:TPU:1, one launch (start us, length us, event | category | flops | bytes accessed | tf_op | source)
XLA Modules:
  0.0 371.3 jit_solution(12669012684862657344)
XLA Ops:
  17.6 8.4 %all-to-all-start = ((bf16[1,128,16,512]{3,1,0,2:T(8,128)(2,1)}), bf16[1,128,16,512]{3,1,0,2:T(8,128)(2,1)S(1)}, u32[]{:S(2)}, u32[]{:S(2)}) async-start(bf16[1,128,16,512]{3,1,0,2:T(8,128)(2,1)} %copy.75), calls=%async_computation | async-start | bytes 4194304 | tf_op jit(solution)/shard_map/all_to_all | solution.py:158
  26.1 30.8 %all-to-all-done = bf16[1,128,16,512]{3,1,0,2:T(8,128)(2,1)S(1)} async-done(((bf16[1,128,16,512]{3,1,0,2:T(8,128)(2,1)}), bf16[1,128,16,512]{3,1,0,2:T(8,128)(2,1)S(1)}, u32[]{:S(2)}, u32[]{:S(2)}) %all-to-all-start) | async-done | bytes 2097184 | tf_op jit(solution)/shard_map/all_to_all | solution.py:158
  67.9 77.8 %while.24 = (s32[]{:T(128)}, f32[2048,128]{1,0:T(8,128)}, f32[2048,128]{1,0:T(8,128)}, f32[4,512,128]{2,1,0:T(8,128)}, s32[4]{0:T(128)S(1)}, /*index=5*/bf16[204...) while((s32[]{:T(128)}, f32[2048,128]{1,0:T(8,128)}, ...), condition=%wide.region_6.7_spmd.clone, body=%wide.region_2.6_spmd.clone.sunk | while | flops 1625815552 | bytes 93731832 | solution.py:131
  73.8 3.2 fusion.134
  91.9 3.2 fusion.134
  97.1 3.2 fusion.135
  102.8 3.1 convolution_add_fusion.2
  111.8 3.2 fusion.134
  117.0 3.2 fusion.135
  122.7 3.1 convolution_add_fusion.2
  131.7 3.2 fusion.134
  136.9 3.2 fusion.135
  145.7 4.9 %fusion.95 = (f32[2048,32]{1,0:T(8,128)}, f32[2048,32]{1,0:T(8,128)}, f32[2048,32]{1,0:T(8,128)}, f32[2048,32]{1,0:T(8,128)S(1)}) fusion(f32[2048,128]{1,0:T(8,128)} %bitcast.71), kind=kLoop, calls=%fused_computation.137 | loop fusion | bytes 2097152 | tf_op jit(solution)/shard_map/while/body/eval_jaxpr/transpose(jvp())/split | solution.py:79
  159.0 4.0 %fusion.63 = (f32[2048,32]{0,1:T(8,128)S(1)}, f32[2048,32]{0,1:T(8,128)S(1)}, f32[2048,32]{0,1:T(8,128)S(1)}, f32[2048,32]{0,1:T(8,128)S(1)}, f32[2048,32]{0,1:T...) fusion(f32[2048,32]{0,1:T(8,128)} %copy.107, f32[2048,32]{0,1:T(8,128)} %copy.108, ...), kind=kLoop, calls=%fused_computation.95 | loop fusion | flops 1966080 | bytes 4210816 | tf_op jit(solution)/shard_map/while/body/eval_jaxpr/transpose(jvp())/add_any | solution.py:77
  168.4 5.7 %copy.87 = bf16[1,2048,1,384]{3,2,0,1:T(2,128)(2,1)} copy(bf16[1,2048,1,384]{1,3,2,0:T(8,128)(2,1)S(1)} %maximum_bitcast_fusion) | data formatting | bytes 3145728 | tf_op jit(solution)/shard_map/transpose;reshape | solution.py:176
  174.6 34.5 %reduce.3 = bf16[2048,384]{1,0:T(8,128)(2,1)S(1)} reduce(bf16[2048,1,1,384]{3,2,1,0:T(2,128)(2,1)} %bitcast.72, bf16[]{:T(256)} %broadcast.219), dimensions={1,2}, to_apply=%bitcast.40.reduce_sub_computation | reduce | bytes 3145730
  210.5 25.3 %all_to_all.43 = bf16[16,2,24576]{2,1,0:T(2,128)(2,1)S(1)} all-to-all(bf16[16,2,24576]{2,1,0:T(2,128)(2,1)} %reshape.148), channel_id=1, replica_groups=mesh['sp'=16,'dp'=8] {'sp'}, dimensions={0} | all-to-all | bytes 3145728 | tf_op jit(solution)/shard_map/all_to_all | solution.py:179
  235.8 6.3 %reshape.149 = bf16[2048,1,1,384]{3,2,1,0:T(2,128)(2,1)} reshape(bf16[16,2,24576]{2,1,0:T(2,128)(2,1)S(1)} %all_to_all.43) | data formatting | bytes 3145728
  245.9 5.5 %convert_bitcast_fusion = bf16[4096,1024]{0,1:T(8,128)(2,1)} fusion(bf16[1,128,4096]{2,1,0:T(8,128)(2,1)S(1)} %copy-done, bf16[128,512]{0,1:T(8,128)(2,1)S(1)} %bitcast.86, bf16[128,512]{0,1:T(8,128)(2,1)S(1)} %bitcast.84), kind=kOutput, calls=%fused_computation.21 | convolution fusion | flops 1078460416 | bytes 9699328 | tf_op jit(solution)/shard_map/dot_general | solution.py:89
  253.8 49.0 %reduce-scatter.2.cloned.1.call-done = bf16[512,1024]{0,1:T(8,128)(2,1)} async-done(((bf16[4096,1024]{0,1:T(8,128)(2,1)}), bf16[512,1024]{0,1:T(8,128)(2,1)}) %reduce-scatter.2.cloned.1.call-update) | async-done | bytes 1048592 | tf_op jit(solution)/shard_map/reduce_scatter | solution.py:202
  304.3 22.3 %all_to_all.44 = bf16[16,32,1024]{2,1,0:T(8,128)(2,1)S(1)} all-to-all(bf16[16,32,1024]{2,1,0:T(8,128)(2,1)S(1)} %bitcast.76), channel_id=1, replica_groups=mesh['sp'=16,'dp'=8] {'sp'}, dimensions={0} | all-to-all | bytes 2097152 | tf_op jit(solution)/shard_map/all_to_all | solution.py:53
  327.9 3.9 %all-to-all-start.3 = ((bf16[16,32,1024]{2,1,0:T(8,128)(2,1)}), bf16[16,32,1024]{2,1,0:T(8,128)(2,1)S(1)}, u32[]{:S(2)}, u32[]{:S(2)}) async-start(bf16[16,32,1024]{2,1,0:T(8,128)(2,1)} %broadcast_in_dim.70), calls=%async_computation.4 | async-start | bytes 2097152 | tf_op jit(solution)/shard_map/all_to_all | solution.py:30
  333.1 22.3 %all-gather.2.cloned.1.call-done = bf16[4096,1024]{1,0:T(8,128)(2,1)} async-done(((bf16[512,1024]{1,0:T(8,128)(2,1)}), bf16[4096,1024]{1,0:T(8,128)(2,1)}) %all-gather.2.cloned.1.call-update) | async-done | bytes 8388624 | tf_op jit(solution)/shard_map/all_gather | solution.py:19
  355.4 7.2 %fusion.13 = bf16[1,128,4096]{2,1,0:T(8,128)(2,1)} fusion(bf16[4096,1024]{1,0:T(8,128)(2,1)} %all-gather.2.cloned.1.call-done, bf16[128,512]{0,1:T(8,128)(2,1)S(1)} %bitcast.87, bf16[128,512]{0,1:T(8,128)(2,1)S(1)} %bitcast.85), kind=kOutput, calls=%fused_computation.23 | convolution fusion | flops 1074790400 | bytes 9699328 | tf_op jit(solution)/shard_map/dot_general | solution.py:83
  (200 shorter events, 95.5 us)
Async XLA Ops:
  7.2 238.7 %copy-start = (bf16[1,128,4096]{2,1,0:T(8,128)(2,1)S(1)}, bf16[1,128,4096]{2,1,0:T(8,128)(2,1)}, u32[]{:S(2)}) copy-start(bf16[1,128,4096]{2,1,0:T(8,128)(2,1)} %param.15) | copy-start | bytes 3145732
  17.6 39.4 %all-to-all-start = ((bf16[1,128,16,512]{3,1,0,2:T(8,128)(2,1)}), bf16[1,128,16,512]{3,1,0,2:T(8,128)(2,1)S(1)}, u32[]{:S(2)}, u32[]{:S(2)}) async-start(bf16[1,128,16,512]{3,1,0,2:T(8,128)(2,1)} %copy.75), calls=%async_computation | async-start | bytes 4194304 | tf_op jit(solution)/shard_map/all_to_all | solution.py:158
  26.0 276.8 %reduce-scatter.2.cloned.1.call-start = ((), (), s32[]{:S(2)}) async-start(), calls=%async_computation.6 | async-start | bytes 9437184 | tf_op jit(solution)/shard_map/reduce_scatter | solution.py:202
  58.3 4.4 %copy-start.21 = (f32[128]{0:T(128)S(1)}, f32[128]{0:T(128)}, u32[]{:S(2)}) copy-start(f32[128]{0:T(128)} %param.19) | copy-start | bytes 1540
  61.1 4.6 %copy-start.8 = (bf16[2048,128]{0,1:T(8,128)(2,1)}, bf16[2048,128]{0,1:T(8,128)(2,1)S(1)}, u32[]{:S(2)}) copy-start(bf16[2048,128]{0,1:T(8,128)(2,1)S(1)} %copy.102) | copy-start | bytes 1572868
  67.9 5.7 %copy-start.15 = (bf16[2048,128]{1,0:T(8,128)(2,1)}, bf16[2048,128]{1,0:T(8,128)(2,1)S(1)}, u32[]{:S(2)}) copy-start(bf16[2048,128]{1,0:T(8,128)(2,1)S(1)} %get-tuple-element.348) | copy-start | bytes 1572868 | tf_op jit(solution)/shard_map/while/body/eval_jaxpr/while
  67.9 5.8 %copy-start.3 = (bf16[2048,128]{1,0:T(8,128)(2,1)}, bf16[2048,128]{1,0:T(8,128)(2,1)S(1)}, u32[]{:S(2)}) copy-start(bf16[2048,128]{1,0:T(8,128)(2,1)S(1)} %get-tuple-element.349) | copy-start | bytes 1572868 | tf_op jit(solution)/shard_map/while/body/eval_jaxpr/while
  73.8 3.5 copy-start.1
  79.0 5.2 %copy-start.2 = (f32[512,2048]{1,0:T(8,128)S(1)}, f32[512,2048]{1,0:T(8,128)}, u32[]{:S(2)}) copy-start(f32[512,2048]{1,0:T(8,128)} %fusion.133) | copy-start | bytes 12582916 | tf_op jit(solution)/shard_map/while/body/eval_jaxpr/while
  86.1 5.7 %copy-start.15 = (bf16[2048,128]{1,0:T(8,128)(2,1)}, bf16[2048,128]{1,0:T(8,128)(2,1)S(1)}, u32[]{:S(2)}) copy-start(bf16[2048,128]{1,0:T(8,128)(2,1)S(1)} %get-tuple-element.348) | copy-start | bytes 1572868 | tf_op jit(solution)/shard_map/while/body/eval_jaxpr/while
  86.1 5.8 %copy-start.3 = (bf16[2048,128]{1,0:T(8,128)(2,1)}, bf16[2048,128]{1,0:T(8,128)(2,1)S(1)}, u32[]{:S(2)}) copy-start(bf16[2048,128]{1,0:T(8,128)(2,1)S(1)} %get-tuple-element.349) | copy-start | bytes 1572868 | tf_op jit(solution)/shard_map/while/body/eval_jaxpr/while
  97.1 5.6 %copy-start.2 = (f32[512,2048]{1,0:T(8,128)S(1)}, f32[512,2048]{1,0:T(8,128)}, u32[]{:S(2)}) copy-start(f32[512,2048]{1,0:T(8,128)} %fusion.133) | copy-start | bytes 12582916 | tf_op jit(solution)/shard_map/while/body/eval_jaxpr/while
  105.9 5.7 %copy-start.15 = (bf16[2048,128]{1,0:T(8,128)(2,1)}, bf16[2048,128]{1,0:T(8,128)(2,1)S(1)}, u32[]{:S(2)}) copy-start(bf16[2048,128]{1,0:T(8,128)(2,1)S(1)} %get-tuple-element.348) | copy-start | bytes 1572868 | tf_op jit(solution)/shard_map/while/body/eval_jaxpr/while
  105.9 5.8 %copy-start.3 = (bf16[2048,128]{1,0:T(8,128)(2,1)}, bf16[2048,128]{1,0:T(8,128)(2,1)S(1)}, u32[]{:S(2)}) copy-start(bf16[2048,128]{1,0:T(8,128)(2,1)S(1)} %get-tuple-element.349) | copy-start | bytes 1572868 | tf_op jit(solution)/shard_map/while/body/eval_jaxpr/while
  117.0 5.6 %copy-start.2 = (f32[512,2048]{1,0:T(8,128)S(1)}, f32[512,2048]{1,0:T(8,128)}, u32[]{:S(2)}) copy-start(f32[512,2048]{1,0:T(8,128)} %fusion.133) | copy-start | bytes 12582916 | tf_op jit(solution)/shard_map/while/body/eval_jaxpr/while
  125.8 5.7 %copy-start.15 = (bf16[2048,128]{1,0:T(8,128)(2,1)}, bf16[2048,128]{1,0:T(8,128)(2,1)S(1)}, u32[]{:S(2)}) copy-start(bf16[2048,128]{1,0:T(8,128)(2,1)S(1)} %get-tuple-element.348) | copy-start | bytes 1572868 | tf_op jit(solution)/shard_map/while/body/eval_jaxpr/while
  125.8 5.8 %copy-start.3 = (bf16[2048,128]{1,0:T(8,128)(2,1)}, bf16[2048,128]{1,0:T(8,128)(2,1)S(1)}, u32[]{:S(2)}) copy-start(bf16[2048,128]{1,0:T(8,128)(2,1)S(1)} %get-tuple-element.349) | copy-start | bytes 1572868 | tf_op jit(solution)/shard_map/while/body/eval_jaxpr/while
  136.9 5.6 %copy-start.2 = (f32[512,2048]{1,0:T(8,128)S(1)}, f32[512,2048]{1,0:T(8,128)}, u32[]{:S(2)}) copy-start(f32[512,2048]{1,0:T(8,128)} %fusion.133) | copy-start | bytes 12582916 | tf_op jit(solution)/shard_map/while/body/eval_jaxpr/while
  150.6 7.1 %copy-start.7 = (f32[2048,128]{1,0:T(8,128)S(1)}, f32[2048,128]{1,0:T(8,128)}, u32[]{:S(2)}) copy-start(f32[2048,128]{1,0:T(8,128)} %get-tuple-element.69) | copy-start | bytes 3145732
  157.7 5.3 %copy-start.11 = (bf16[2048,128]{0,1:T(8,128)(2,1)S(1)}, bf16[2048,128]{0,1:T(8,128)(2,1)}, u32[]{:S(2)}) copy-start(bf16[2048,128]{0,1:T(8,128)(2,1)} %copy-done.10) | copy-start | bytes 1572868
  159.0 4.5 %copy-start.9 = (bf16[2048,128]{0,1:T(8,128)(2,1)S(1)}, bf16[2048,128]{0,1:T(8,128)(2,1)}, u32[]{:S(2)}) copy-start(bf16[2048,128]{0,1:T(8,128)(2,1)} %copy-done.8) | copy-start | bytes 1572868
  251.5 103.9 %all-gather.2.cloned.1.call-start = ((), (), s32[]{:S(2)}) async-start(), calls=%async_computation.5 | async-start | bytes 9437184 | tf_op jit(solution)/shard_map/all_gather | solution.py:19
  326.6 5.2 %copy-start.17 = (bf16[1,128,16,128]{3,1,2,0:T(8,128)(2,1)S(1)}, bf16[1,128,16,128]{3,1,2,0:T(8,128)(2,1)}, u32[]{:S(2)}) copy-start(bf16[1,128,16,128]{3,1,2,0:T(8,128)(2,1)} %get-tuple-element.217) | copy-start | bytes 1572868
  327.9 34.7 %all-to-all-start.3 = ((bf16[16,32,1024]{2,1,0:T(8,128)(2,1)}), bf16[16,32,1024]{2,1,0:T(8,128)(2,1)S(1)}, u32[]{:S(2)}, u32[]{:S(2)}) async-start(bf16[16,32,1024]{2,1,0:T(8,128)(2,1)} %broadcast_in_dim.70), calls=%async_computation.4 | async-start | bytes 2097152 | tf_op jit(solution)/shard_map/all_to_all | solution.py:30
  (32 other events, 87.6 us)
Sparse Core Ops, SparseCore 0:
  251.6 51.1 reduce-scatter.1
  305.1 50.2 all-gather.1
where the time goes:
time: 373 us; the launch traced here: 371 us
  waiting for transfers between devices  102 us (27%)
  matrix products  69.1 us (19%)
  other arithmetic  63.2 us (17%)
  local copies, waits for them, and re-layouts  59.7 us (16%)
  blocking collectives  47.5 us (13%)
  between operations  14.4 us (4%)
  starting transfers between devices  12.4 us (3%)
    reduce_scatter x1, waiting for transfers between devices, on_device(): lax.psum_scatter(contract_rows(flat_in, kv_grad).astype(jnp.bfloat16), 'd...  49 us
    unnamed x3, other arithmetic  34.5 us
    all_to_all x1, waiting for transfers between devices, on_device(): lax.all_to_all(bundle, 'sp', split_axis=2, concat_axis=1, tiled=True)  30.8 us
    dot_general x9, matrix products, contract_rows(): lax.dot_general(left_side, right_side, (((0,), (0,)), ((), ())), preferre...  28.9 us
    unnamed x38, local copies, waits for them, and re-layouts  27.8 us
    all_to_all x1, blocking collectives, on_device(): lax.all_to_all(head_out, 'sp', split_axis=1, concat_axis=2, tiled=True)  25.3 us
    all_to_all x1, blocking collectives, sum_at_owner(): parts = lax.all_to_all(cut_along(array, dim, peers), axis, 0, 0, tiled=True)  22.3 us
    all_gather x1, waiting for transfers between devices, sent_together(): result = lax.all_gather(both, axis, axis=dim, tiled=True)  22.3 us
  transfers between devices with their start and end apart: 4, of which 3 were waited for; matrix products, arithmetic and copies ran while one was open for 3% of the time, Pallas kernels for 0%

commit v1 on v0

--- a/solution.py
+++ b/solution.py
@@ -176,7 +176,15 @@
     head_out = all_grads.reshape(arrived_seqs, head_count, length, 3 * HEAD_DIM).transpose(
         0, 2, 1, 3
     )
-    token_grads = lax.all_to_all(head_out, "sp", split_axis=1, concat_axis=2, tiled=True)
+    token_grads = jnp.concatenate(
+        lax.all_to_all(
+            jnp.stack(jnp.split(head_out, lax.axis_size("sp"), axis=1)),
+            concat_axis=0,
+            axis_name="sp",
+            split_axis=0,
+        ),
+        axis=2,
+    )
     grad_query = token_grads[:, :, :, :HEAD_DIM].reshape(seq_count, tokens_here, HEADS * HEAD_DIM)
 
     def grouped(array):

time: 373 us -> 318 us (0.85)
  other arithmetic: 63.2 us -> 26.4 us
  local copies, waits for them, and re-layouts: 59.7 us -> 41.1 us
    unnamed x3 -> x2, other arithmetic: 34.5 us -> 0.01 us
    unnamed x38 -> x49, local copies, waits for them, and re-layouts: 27.8 us -> 17.5 us
    another operation x1, local copies, waits for them, and re-layouts: 5.66 us -> 0.05 us  [on_device(): jnp.stack(jnp.split(head_out, lax.axis_size('sp'), axis=1))]
  transfers between devices with their start and end apart: 4 -> 4, of which waited for: 3 -> 3; matrix products, arithmetic and copies ran while one was open for 3% -> 4% of each run, Pallas kernels for 0% -> 0%
where the time goes in v1:
time: 318 us; the launch traced here: 317 us
  waiting for transfers between devices  103 us (32%)
  matrix products  69.1 us (22%)
  blocking collectives  47.4 us (15%)
  local copies, waits for them, and re-layouts  41.1 us (13%)
  other arithmetic  26.4 us (8%)
  between operations  14.4 us (5%)
  starting transfers between devices  12.2 us (4%)
  loops' own time  3.3 us (1%)
    reduce_scatter x1, waiting for transfers between devices, on_device(): lax.psum_scatter(contract_rows(flat_in, kv_grad).astype(jnp.bfloat16), 'd...  49 us
    all_to_all x1, waiting for transfers between devices, on_device(): lax.all_to_all(bundle, 'sp', split_axis=2, concat_axis=1, tiled=True)  30.8 us
    dot_general x9, matrix products, contract_rows(): lax.dot_general(left_side, right_side, (((0,), (0,)), ((), ())), preferre...  28.9 us
    all_to_all x1, blocking collectives, on_device(): lax.all_to_all(jnp.stack(jnp.split(head_out, lax.axis_size('sp'), axis=1)...  25.1 us
    all_gather x1, waiting for transfers between devices, sent_together(): result = lax.all_gather(both, axis, axis=dim, tiled=True)  22.8 us
    all_to_all x1, blocking collectives, sum_at_owner(): parts = lax.all_to_all(cut_along(array, dim, peers), axis, 0, 0, tiled=True)  22.3 us
    dot_general x9, matrix products, contract_cols(): lax.dot_general(left_side, right_side, (((1,), (1,)), ((), ())), preferre...  17.6 us
    unnamed x49, local copies, waits for them, and re-layouts  17.5 us
  transfers between devices with their start and end apart: 4, of which 3 were waited for; matrix products, arithmetic and copies ran while one was open for 4% of the time, Pallas kernels for 0%

profile of v1, /device:TPU:1, one launch (start us, length us, event | category | flops | bytes accessed | tf_op | source)
XLA Modules:
  0.0 316.5 jit_solution(3671656724658698648)
XLA Ops:
  17.6 8.4 %all-to-all-start = ((bf16[1,128,16,512]{3,1,0,2:T(8,128)(2,1)}), bf16[1,128,16,512]{3,1,0,2:T(8,128)(2,1)S(1)}, u32[]{:S(2)}, u32[]{:S(2)}) async-start(bf16[1,128,16,512]{3,1,0,2:T(8,128)(2,1)} %copy.45), calls=%async_computation | async-start | bytes 4194304 | tf_op jit(solution)/shard_map/all_to_all | solution.py:158
  26.1 30.8 %all-to-all-done = bf16[1,128,16,512]{3,1,0,2:T(8,128)(2,1)S(1)} async-done(((bf16[1,128,16,512]{3,1,0,2:T(8,128)(2,1)}), bf16[1,128,16,512]{3,1,0,2:T(8,128)(2,1)S(1)}, u32[]{:S(2)}, u32[]{:S(2)}) %all-to-all-start) | async-done | bytes 2097184 | tf_op jit(solution)/shard_map/all_to_all | solution.py:158
  67.9 78.6 %while.24 = (s32[]{:T(128)}, f32[2048,128]{1,0:T(8,128)}, f32[2048,128]{1,0:T(8,128)}, f32[4,512,128]{2,1,0:T(8,128)}, s32[4]{0:T(128)S(1)}, /*index=5*/bf16[204...) while((s32[]{:T(128)}, f32[2048,128]{1,0:T(8,128)}, ...), condition=%wide.region_6.7_spmd.clone, body=%wide.region_2.6_spmd.clone.sunk | while | flops 1625815552 | bytes 93731832 | solution.py:131
  71.1 2.8 fusion.149
  74.0 3.2 %fusion.150 = f32[512]{0:T(512)S(1)} fusion(bf16[2048,128]{1,0:T(8,128)(2,1)S(1)} %get-tuple-element.310, f32[512,2048]{1,0:T(8,128)} %fusion.149, bf16[512,128]{0,1:T(8,128)(2,1)S(1)} %copy.79), kind=kOutput, calls=%fused_computation.12.clone.1 | convolution fusion | flops 269680128 | bytes 4851712 | tf_op jit(solution)/shard_map/while/body/eval_jaxpr/while/body/eval_jaxpr/dot_general | solution.py:121
  79.2 2.8 fusion.151
  92.3 3.2 %fusion.150 = f32[512]{0:T(512)S(1)} fusion(bf16[2048,128]{1,0:T(8,128)(2,1)S(1)} %get-tuple-element.310, f32[512,2048]{1,0:T(8,128)} %fusion.149, bf16[512,128]{0,1:T(8,128)(2,1)S(1)} %copy.79), kind=kOutput, calls=%fused_computation.12.clone.1 | convolution fusion | flops 269680128 | bytes 4851712 | tf_op jit(solution)/shard_map/while/body/eval_jaxpr/while/body/eval_jaxpr/dot_general | solution.py:121
  97.5 3.2 fusion.151
  103.2 3.1 convolution_add_fusion.2
  112.4 3.2 %fusion.150 = f32[512]{0:T(512)S(1)} fusion(bf16[2048,128]{1,0:T(8,128)(2,1)S(1)} %get-tuple-element.310, f32[512,2048]{1,0:T(8,128)} %fusion.149, bf16[512,128]{0,1:T(8,128)(2,1)S(1)} %copy.79), kind=kOutput, calls=%fused_computation.12.clone.1 | convolution fusion | flops 269680128 | bytes 4851712 | tf_op jit(solution)/shard_map/while/body/eval_jaxpr/while/body/eval_jaxpr/dot_general | solution.py:121
  117.6 3.2 fusion.151
  123.3 3.1 convolution_add_fusion.2
  132.5 3.2 %fusion.150 = f32[512]{0:T(512)S(1)} fusion(bf16[2048,128]{1,0:T(8,128)(2,1)S(1)} %get-tuple-element.310, f32[512,2048]{1,0:T(8,128)} %fusion.149, bf16[512,128]{0,1:T(8,128)(2,1)S(1)} %copy.79), kind=kOutput, calls=%fused_computation.12.clone.1 | convolution fusion | flops 269680128 | bytes 4851712 | tf_op jit(solution)/shard_map/while/body/eval_jaxpr/while/body/eval_jaxpr/dot_general | solution.py:121
  137.7 3.2 fusion.151
  143.4 3.1 convolution_add_fusion.2
  146.5 4.6 %fusion.111 = (f32[2048,32]{1,0:T(8,128)}, f32[2048,32]{1,0:T(8,128)}, f32[2048,32]{1,0:T(8,128)S(1)}, f32[2048,32]{1,0:T(8,128)S(1)}) fusion(f32[2048,128]{1,0:T(8,128)} %bitcast.131), kind=kLoop, calls=%fused_computation.169 | loop fusion | bytes 2097152 | tf_op jit(solution)/shard_map/while/body/eval_jaxpr/transpose(jvp())/split | solution.py:79
  157.3 3.7 %fusion.63 = (f32[2048,32]{0,1:T(8,128)S(1)}, f32[2048,32]{0,1:T(8,128)S(1)}, f32[2048,32]{0,1:T(8,128)S(1)}, f32[2048,32]{0,1:T(8,128)S(1)}, f32[2048,32]{0,1:T...) fusion(f32[2048,32]{0,1:T(8,128)} %copy.75, f32[2048,32]{0,1:T(8,128)} %copy.76, ...), kind=kLoop, calls=%fused_computation.95 | loop fusion | flops 1966080 | bytes 4210816 | tf_op jit(solution)/shard_map/while/body/eval_jaxpr/transpose(jvp())/add_any | solution.py:77
  164.9 25.1 %all_to_all.30 = bf16[16,1,128,1,384]{2,4,3,1,0:T(8,128)(2,1)S(1)} all-to-all(bf16[16,1,128,1,384]{2,4,3,1,0:T(8,128)(2,1)S(1)} %fusion.79), channel_id=1, replica_groups=mesh['sp'=16,'dp'=8] {'sp'}, dimensions={0} | all-to-all | bytes 3145728 | tf_op jit(solution)/shard_map/all_to_all | solution.py:180
  191.1 5.6 %convert_bitcast_fusion = bf16[4096,1024]{0,1:T(8,128)(2,1)} fusion(bf16[1,128,4096]{2,1,0:T(8,128)(2,1)S(1)} %copy-done, bf16[128,512]{0,1:T(8,128)(2,1)S(1)} %bitcast.144, bf16[128,512]{0,1:T(8,128)(2,1)S(1)} %bitcast.142), kind=kOutput, calls=%fused_computation.21 | convolution fusion | flops 1078460416 | bytes 9699328 | tf_op jit(solution)/shard_map/dot_general | solution.py:89
  199.0 49.0 %reduce-scatter.2.cloned.1.call-done = bf16[512,1024]{0,1:T(8,128)(2,1)} async-done(((bf16[4096,1024]{0,1:T(8,128)(2,1)}), bf16[512,1024]{0,1:T(8,128)(2,1)}) %reduce-scatter.2.cloned.1.call-update) | async-done | bytes 1048592 | tf_op jit(solution)/shard_map/reduce_scatter | solution.py:210
  249.5 22.3 %all_to_all.31 = bf16[16,32,1024]{2,1,0:T(8,128)(2,1)S(1)} all-to-all(bf16[16,32,1024]{2,1,0:T(8,128)(2,1)S(1)} %bitcast.134), channel_id=1, replica_groups=mesh['sp'=16,'dp'=8] {'sp'}, dimensions={0} | all-to-all | bytes 2097152 | tf_op jit(solution)/shard_map/all_to_all | solution.py:53
  273.1 3.7 %all-to-all-start.3 = ((bf16[16,32,1024]{2,1,0:T(8,128)(2,1)}), bf16[16,32,1024]{2,1,0:T(8,128)(2,1)S(1)}, u32[]{:S(2)}, u32[]{:S(2)}) async-start(bf16[16,32,1024]{2,1,0:T(8,128)(2,1)} %broadcast_in_dim.70), calls=%async_computation.4 | async-start | bytes 2097152 | tf_op jit(solution)/shard_map/all_to_all | solution.py:30
  277.8 22.8 %all-gather.2.cloned.1.call-done = bf16[4096,1024]{1,0:T(8,128)(2,1)} async-done(((bf16[512,1024]{1,0:T(8,128)(2,1)}), bf16[4096,1024]{1,0:T(8,128)(2,1)}) %all-gather.2.cloned.1.call-update) | async-done | bytes 8388624 | tf_op jit(solution)/shard_map/all_gather | solution.py:19
  300.6 7.3 %fusion.13 = bf16[1,128,4096]{2,1,0:T(8,128)(2,1)} fusion(bf16[4096,1024]{1,0:T(8,128)(2,1)} %all-gather.2.cloned.1.call-done, bf16[128,512]{0,1:T(8,128)(2,1)S(1)} %bitcast.145, bf16[128,512]{0,1:T(8,128)(2,1)S(1)} %bitcast.143), kind=kOutput, calls=%fused_computation.23 | convolution fusion | flops 1074790400 | bytes 9699328 | tf_op jit(solution)/shard_map/dot_general | solution.py:83
  (207 shorter events, 78.5 us)
Async XLA Ops:
  7.2 184.0 %copy-start = (bf16[1,128,4096]{2,1,0:T(8,128)(2,1)S(1)}, bf16[1,128,4096]{2,1,0:T(8,128)(2,1)}, u32[]{:S(2)}) copy-start(bf16[1,128,4096]{2,1,0:T(8,128)(2,1)} %param.15) | copy-start | bytes 3145732
  17.6 39.4 %all-to-all-start = ((bf16[1,128,16,512]{3,1,0,2:T(8,128)(2,1)}), bf16[1,128,16,512]{3,1,0,2:T(8,128)(2,1)S(1)}, u32[]{:S(2)}, u32[]{:S(2)}) async-start(bf16[1,128,16,512]{3,1,0,2:T(8,128)(2,1)} %copy.45), calls=%async_computation | async-start | bytes 4194304 | tf_op jit(solution)/shard_map/all_to_all | solution.py:158
  26.0 222.0 %reduce-scatter.2.cloned.1.call-start = ((), (), s32[]{:S(2)}) async-start(), calls=%async_computation.6 | async-start | bytes 9437184 | tf_op jit(solution)/shard_map/reduce_scatter | solution.py:210
  67.9 5.9 %copy-start.15 = (bf16[2048,128]{1,0:T(8,128)(2,1)}, bf16[2048,128]{1,0:T(8,128)(2,1)S(1)}, u32[]{:S(2)}) copy-start(bf16[2048,128]{1,0:T(8,128)(2,1)S(1)} %get-tuple-element.309) | copy-start | bytes 1572868 | tf_op jit(solution)/shard_map/while/body/eval_jaxpr/while
  67.9 6.0 %copy-start.3 = (bf16[2048,128]{1,0:T(8,128)(2,1)}, bf16[2048,128]{1,0:T(8,128)(2,1)S(1)}, u32[]{:S(2)}) copy-start(bf16[2048,128]{1,0:T(8,128)(2,1)S(1)} %get-tuple-element.310) | copy-start | bytes 1572868 | tf_op jit(solution)/shard_map/while/body/eval_jaxpr/while
  74.0 3.5 %copy-start.1 = (f32[512,2048]{1,0:T(8,128)S(1)}, f32[512,2048]{1,0:T(8,128)}, u32[]{:S(2)}) copy-start(f32[512,2048]{1,0:T(8,128)} %fusion.149) | copy-start | bytes 12582916 | tf_op jit(solution)/shard_map/while/body/eval_jaxpr/while
  79.2 5.2 %copy-start.2 = (f32[512,2048]{1,0:T(8,128)S(1)}, f32[512,2048]{1,0:T(8,128)}, u32[]{:S(2)}) copy-start(f32[512,2048]{1,0:T(8,128)} %fusion.149) | copy-start | bytes 12582916 | tf_op jit(solution)/shard_map/while/body/eval_jaxpr/while
  86.3 5.9 %copy-start.15 = (bf16[2048,128]{1,0:T(8,128)(2,1)}, bf16[2048,128]{1,0:T(8,128)(2,1)S(1)}, u32[]{:S(2)}) copy-start(bf16[2048,128]{1,0:T(8,128)(2,1)S(1)} %get-tuple-element.309) | copy-start | bytes 1572868 | tf_op jit(solution)/shard_map/while/body/eval_jaxpr/while
  86.3 6.0 %copy-start.3 = (bf16[2048,128]{1,0:T(8,128)(2,1)}, bf16[2048,128]{1,0:T(8,128)(2,1)S(1)}, u32[]{:S(2)}) copy-start(bf16[2048,128]{1,0:T(8,128)(2,1)S(1)} %get-tuple-element.310) | copy-start | bytes 1572868 | tf_op jit(solution)/shard_map/while/body/eval_jaxpr/while
  92.3 3.5 %copy-start.1 = (f32[512,2048]{1,0:T(8,128)S(1)}, f32[512,2048]{1,0:T(8,128)}, u32[]{:S(2)}) copy-start(f32[512,2048]{1,0:T(8,128)} %fusion.149) | copy-start | bytes 12582916 | tf_op jit(solution)/shard_map/while/body/eval_jaxpr/while
  97.5 5.6 %copy-start.2 = (f32[512,2048]{1,0:T(8,128)S(1)}, f32[512,2048]{1,0:T(8,128)}, u32[]{:S(2)}) copy-start(f32[512,2048]{1,0:T(8,128)} %fusion.149) | copy-start | bytes 12582916 | tf_op jit(solution)/shard_map/while/body/eval_jaxpr/while
  106.4 5.9 %copy-start.15 = (bf16[2048,128]{1,0:T(8,128)(2,1)}, bf16[2048,128]{1,0:T(8,128)(2,1)S(1)}, u32[]{:S(2)}) copy-start(bf16[2048,128]{1,0:T(8,128)(2,1)S(1)} %get-tuple-element.309) | copy-start | bytes 1572868 | tf_op jit(solution)/shard_map/while/body/eval_jaxpr/while
  106.4 6.0 %copy-start.3 = (bf16[2048,128]{1,0:T(8,128)(2,1)}, bf16[2048,128]{1,0:T(8,128)(2,1)S(1)}, u32[]{:S(2)}) copy-start(bf16[2048,128]{1,0:T(8,128)(2,1)S(1)} %get-tuple-element.310) | copy-start | bytes 1572868 | tf_op jit(solution)/shard_map/while/body/eval_jaxpr/while
  112.4 3.5 %copy-start.1 = (f32[512,2048]{1,0:T(8,128)S(1)}, f32[512,2048]{1,0:T(8,128)}, u32[]{:S(2)}) copy-start(f32[512,2048]{1,0:T(8,128)} %fusion.149) | copy-start | bytes 12582916 | tf_op jit(solution)/shard_map/while/body/eval_jaxpr/while
  117.6 5.6 %copy-start.2 = (f32[512,2048]{1,0:T(8,128)S(1)}, f32[512,2048]{1,0:T(8,128)}, u32[]{:S(2)}) copy-start(f32[512,2048]{1,0:T(8,128)} %fusion.149) | copy-start | bytes 12582916 | tf_op jit(solution)/shard_map/while/body/eval_jaxpr/while
  126.4 5.9 %copy-start.15 = (bf16[2048,128]{1,0:T(8,128)(2,1)}, bf16[2048,128]{1,0:T(8,128)(2,1)S(1)}, u32[]{:S(2)}) copy-start(bf16[2048,128]{1,0:T(8,128)(2,1)S(1)} %get-tuple-element.309) | copy-start | bytes 1572868 | tf_op jit(solution)/shard_map/while/body/eval_jaxpr/while
  126.5 6.0 %copy-start.3 = (bf16[2048,128]{1,0:T(8,128)(2,1)}, bf16[2048,128]{1,0:T(8,128)(2,1)S(1)}, u32[]{:S(2)}) copy-start(bf16[2048,128]{1,0:T(8,128)(2,1)S(1)} %get-tuple-element.310) | copy-start | bytes 1572868 | tf_op jit(solution)/shard_map/while/body/eval_jaxpr/while
  132.5 3.5 %copy-start.1 = (f32[512,2048]{1,0:T(8,128)S(1)}, f32[512,2048]{1,0:T(8,128)}, u32[]{:S(2)}) copy-start(f32[512,2048]{1,0:T(8,128)} %fusion.149) | copy-start | bytes 12582916 | tf_op jit(solution)/shard_map/while/body/eval_jaxpr/while
  137.7 5.6 %copy-start.2 = (f32[512,2048]{1,0:T(8,128)S(1)}, f32[512,2048]{1,0:T(8,128)}, u32[]{:S(2)}) copy-start(f32[512,2048]{1,0:T(8,128)} %fusion.149) | copy-start | bytes 12582916 | tf_op jit(solution)/shard_map/while/body/eval_jaxpr/while
  151.4 5.6 %copy-start.7 = (f32[2048,128]{1,0:T(8,128)S(1)}, f32[2048,128]{1,0:T(8,128)}, u32[]{:S(2)}) copy-start(f32[2048,128]{1,0:T(8,128)} %get-tuple-element.69) | copy-start | bytes 3145732
  157.3 3.8 %copy-start.11 = (bf16[2048,128]{0,1:T(8,128)(2,1)S(1)}, bf16[2048,128]{0,1:T(8,128)(2,1)}, u32[]{:S(2)}) copy-start(bf16[2048,128]{0,1:T(8,128)(2,1)} %copy-done.10) | copy-start | bytes 1572868
  196.7 103.9 %all-gather.2.cloned.1.call-start = ((), (), s32[]{:S(2)}) async-start(), calls=%async_computation.5 | async-start | bytes 9437184 | tf_op jit(solution)/shard_map/all_gather | solution.py:19
  271.8 5.0 %copy-start.17 = (bf16[1,128,16,128]{1,3,2,0:T(8,128)(2,1)S(1)}, bf16[1,128,16,128]{1,3,2,0:T(8,128)(2,1)}, u32[]{:S(2)}) copy-start(bf16[1,128,16,128]{1,3,2,0:T(8,128)(2,1)} %get-tuple-element.178) | copy-start | bytes 1572868
  273.1 34.8 %all-to-all-start.3 = ((bf16[16,32,1024]{2,1,0:T(8,128)(2,1)}), bf16[16,32,1024]{2,1,0:T(8,128)(2,1)S(1)}, u32[]{:S(2)}, u32[]{:S(2)}) async-start(bf16[16,32,1024]{2,1,0:T(8,128)(2,1)} %broadcast_in_dim.70), calls=%async_computation.4 | async-start | bytes 2097152 | tf_op jit(solution)/shard_map/all_to_all | solution.py:30
  (32 other events, 76.8 us)
Sparse Core Ops, SparseCore 0:
  196.8 51.1 reduce-scatter.1
  250.3 50.2 all-gather.1
